TPU v7x, 32 devices: a whole 2x2x4 slice. The times are simulated.
32 devices in a mesh: sp: 16 (over z, y, x), tp: 2 (over core).
Axes of the slice: x: 2, y: 2, z: 4, core: 2. Of those that a mesh axis runs over, the one named last changes fastest.
Arguments:
- queries: bfloat16 [3072, 1024], P('sp', 'tp'), may hold values from -6 to 6
- keys: bfloat16 [3072, 512], P('sp', 'tp'), may hold values from -6 to 6
- values: bfloat16 [3072, 512], P('sp', 'tp'), may hold values from -6 to 6
- query_gain: float32 [16, 64], P('tp'), may hold values from 1.4 to 7.5
- key_gain: float32 [8, 64], P('tp'), may hold values from 1.4 to 7.5
- out_weight: bfloat16 [1024, 2048], P('tp'), may hold values from -0.375 to 0.375
- residual: bfloat16 [3072, 2048], P('sp'), may hold values from -170 to 170
- norm_gain: float32 [2048], replicated, may hold values from 0.1 to 1.9
- gate_weight: bfloat16 [2048, 5632], P('sp', 'tp'), may hold values from -0.125 to 0.125
- up_weight: bfloat16 [2048, 5632], P('sp', 'tp'), may hold values from -0.125 to 0.125
- down_weight: bfloat16 [5632, 2048], P('tp', 'sp'), may hold values from -0.15625 to 0.15625
Outputs:
- mixed: bfloat16 [3072, 2048], P('sp')
All inputs are finite; a program needn't handle non-finite values.
Results may differ from a plain program's by a relative error of at most 0.017.
Values may be sent and summed in bfloat16 or wider, within the bound.
A program may use at most 128 MiB of HBM per device.

v0:
```python
import jax
import jax.numpy as jnp
from jax import lax
from jax.sharding import PartitionSpec as P

GRID_W = 64


epsilon = 1e-06
rope_base = 10000.0
block_keys = 2048


def rotate_pairs(entries, places):
    half = entries.shape[-1] // 2
    frequency = rope_base ** (-jnp.arange(half, dtype=jnp.float32) / half)
    angle = places.astype(jnp.float32)[:, None, None] * frequency[None, None, :]
    cosine = jnp.cos(angle)
    sine = jnp.sin(angle)
    first = entries[..., :half]
    second = entries[..., half:]
    return jnp.concatenate(
        [first * cosine - second * sine, first * sine + second * cosine], axis=-1
    )


def grid_rotate(entries, grid_rows, grid_cols):
    half = entries.shape[-1] // 2
    return jnp.concatenate(
        [
            rotate_pairs(entries[..., :half], grid_rows),
            rotate_pairs(entries[..., half:], grid_cols),
        ],
        axis=-1,
    )


def head_norm(entries, gains):
    factor = lax.rsqrt(jnp.mean(entries * entries, axis=-1, keepdims=True) + epsilon)
    return entries * factor * gains[None]


def row_norm(mid, norm_gain):
    wide = mid.astype(jnp.float32)
    return (
        wide * lax.rsqrt(jnp.mean(wide * wide, axis=-1, keepdims=True) + epsilon) * norm_gain
    ).astype(jnp.bfloat16)


def block_span(length):
    if length <= block_keys:
        return length
    span = block_keys
    while length % span != 0:
        span = span - 1
    return span


def body(
    queries,
    keys,
    values,
    query_gain,
    key_gain,
    out_weight,
    residual,
    norm_gain,
    gate_weight,
    up_weight,
    down_weight,
):
    own = queries.shape[0]
    heads = query_gain.shape[0]
    key_heads = key_gain.shape[0]
    head_size = query_gain.shape[1]
    group = heads // key_heads
    gate_full, up_full, down_full = (
        lax.all_gather(gate_weight, "sp", axis=0, tiled=True),
        lax.all_gather(up_weight, "sp", axis=0, tiled=True),
        lax.all_gather(down_weight, "sp", axis=1, tiled=True),
    )
    places = lax.axis_index("sp") * own + jnp.arange(own, dtype=jnp.int32)
    grid_rows = places // GRID_W
    grid_cols = places % GRID_W
    query_turned = grid_rotate(
        head_norm(queries.astype(jnp.float32).reshape(own, heads, head_size), query_gain),
        grid_rows,
        grid_cols,
    ).astype(jnp.bfloat16)
    query_groups = query_turned.reshape(own, key_heads, group, head_size)
    key_turned = (
        grid_rotate(
            head_norm(keys.astype(jnp.float32).reshape(own, key_heads, head_size), key_gain),
            grid_rows,
            grid_cols,
        )
        .astype(jnp.bfloat16)
        .reshape(own, key_heads * head_size)
    )
    scale = head_size ** (-0.5)

    def absorb(carry, key_block, value_block):
        top, total, summed = carry
        key_block = key_block.reshape(-1, key_heads, head_size)
        value_block = value_block.reshape(-1, key_heads, head_size)
        score = (
            jnp.einsum(
                "qgrd,kgd->qgrk", query_groups, key_block, preferred_element_type=jnp.float32
            )
            * scale
        )
        new_top = jnp.maximum(top, jnp.max(score, axis=-1))
        weight = jnp.exp(score - new_top[..., None])
        shrink = jnp.exp(top - new_top)
        total = total * shrink + jnp.sum(weight, axis=-1)
        summed = summed * shrink[..., None] + jnp.einsum(
            "qgrk,kgd->qgrd",
            weight.astype(jnp.bfloat16),
            value_block,
            preferred_element_type=jnp.float32,
        )
        return (new_top, total, summed)

    def fold_keys(carry, pieces):
        length = pieces[0].shape[0]
        span = block_span(length)
        if span == length:
            return absorb(carry, pieces[0], pieces[1])
        width = pieces[0].shape[1]
        key_blocks = pieces[0].reshape(length // span, span, width)
        value_blocks = pieces[1].reshape(length // span, span, width)

        def scan_step(inner, blocks):
            return (absorb(inner, blocks[0], blocks[1]), None)

        result, unused = lax.scan(scan_step, carry, (key_blocks, value_blocks))
        return result

    start_state = (
        jnp.full((own, key_heads, group), -jnp.inf, jnp.float32),
        jnp.zeros((own, key_heads, group), jnp.float32),
        jnp.zeros((own, key_heads, group, head_size), jnp.float32),
    )
    top, total, summed = fold_keys(
        start_state,
        (
            lax.all_gather(key_turned, "sp", axis=0, tiled=True),
            lax.all_gather(values, "sp", axis=0, tiled=True),
        ),
    )
    attended = (summed / total[..., None]).reshape(own, heads * head_size).astype(jnp.bfloat16)
    part_rows = own // lax.axis_size("tp")
    branch = lax.psum_scatter(
        jnp.dot(
            lax.slice_in_dim(attended, 0, lax.axis_size("tp") * part_rows, axis=0),
            out_weight,
            preferred_element_type=jnp.float32,
        ).astype(jnp.bfloat16),
        "tp",
        scatter_dimension=0,
        tiled=True,
    ).astype(jnp.float32)
    own_rows = lax.dynamic_slice_in_dim(residual, lax.axis_index("tp") * part_rows, part_rows, 0)
    mid = (own_rows.astype(jnp.float32) + branch).astype(jnp.bfloat16)
    normed_all = lax.all_gather(row_norm(mid, norm_gain), "tp", axis=0, tiled=True)
    gate = jnp.dot(normed_all, gate_full, preferred_element_type=jnp.float32)
    up_value = jnp.dot(normed_all, up_full, preferred_element_type=jnp.float32)
    hidden = (jax.nn.silu(gate) * up_value).astype(jnp.bfloat16)
    terms = jnp.dot(hidden, down_full, preferred_element_type=jnp.float32)
    ffn = lax.psum_scatter(
        terms.astype(jnp.bfloat16), "tp", scatter_dimension=0, tiled=True
    ).astype(jnp.float32)
    finished = (mid.astype(jnp.float32) + ffn).astype(jnp.bfloat16)
    return lax.all_gather(finished, "tp", axis=0, tiled=True)


def solution(mesh):
    in_specs = (
        P("sp", "tp"),
        P("sp", "tp"),
        P("sp", "tp"),
        P("tp", None),
        P("tp", None),
        P("tp", None),
        P("sp", None),
        P(),
        P("sp", "tp"),
        P("sp", "tp"),
        P("tp", "sp"),
    )
    out_specs = P("sp", None)
    return jax.shard_map(body, mesh=mesh, in_specs=in_specs, out_specs=out_specs, check_vma=False)
```

profile of v0, /device:TPU:0, one launch (start us, length us, event | category | flops | bytes accessed | tf_op | source)
XLA Modules:
  0.0 684.2 jit_solution(15495165526293549305)
XLA Ops:
  6.6 1.1 copy.22
  7.8 0.8 fusion.22
  10.4 1.1 copy.24
  11.6 0.8 fusion.20
  13.3 57.5 %all-gather.6.cloned.1.call-done = bf16[3072,256]{1,0:T(8,128)(2,1)} async-done(((bf16[192,256]{1,0:T(8,128)(2,1)}), bf16[3072,256]{1,0:T(8,128)(2,1)}) %all-gather.6.cloned.1.call-update) | async-done | bytes 1572880 | tf_op jit(solution)/shard_map/all_gather | solution.py:147
  70.8 59.5 %all-gather.8.cloned.1.call-done = bf16[3072,256]{1,0:T(8,128)(2,1)} async-done(((bf16[192,256]{1,0:T(8,128)(2,1)}), bf16[3072,256]{1,0:T(8,128)(2,1)}) %all-gather.8.cloned.1.call-update) | async-done | bytes 1572880 | tf_op jit(solution)/shard_map/all_gather | solution.py:148
  130.3 43.6 %while.15 = (s32[]{:T(128)}, f32[192,4,2]{0,2,1:T(2,128)S(1)}, f32[192,4,2]{0,2,1:T(2,128)S(1)}, f32[192,4,2,64]{0,3,2,1:T(8,128)S(1)}, bf16[2,1536,256]{2,1,0:T...) while((s32[]{:T(128)}, f32[192,4,2]{0,2,1:T(2,128)S(1)}, ...), condition=%wide.region_5.6_spmd.clone, body=%wide.region_2.5_spmd.clone.sunk | while | flops 623156736 | bytes 37257324 | solution.py:136
  130.3 2.6 constant_dynamic-slice_fusion.3
  132.9 1.4 copy.33
  134.3 6.0 bitcast_reduce_fusion.2
  140.4 5.4 fusion.51
  145.8 1.4 copy.34
  147.2 4.8 fusion.53
  152.1 2.6 constant_dynamic-slice_fusion.3
  154.7 1.4 copy.33
  156.1 6.0 bitcast_reduce_fusion.2
  162.1 5.4 fusion.51
  167.6 1.4 copy.34
  169.0 4.8 fusion.53
  173.9 1.5 convolution_convert_fusion.1
  177.2 5.2 reduce-scatter.3.cloned.1.call-done
  182.5 1.4 fusion.15
  184.0 2.5 all_gather.23
  186.6 141.1 %all-gather.10.cloned.1.call-done = bf16[2048,2816]{1,0:T(8,128)(2,1)} async-done(((bf16[128,2816]{1,0:T(8,128)(2,1)}), bf16[2048,2816]{1,0:T(8,128)(2,1)}) %all-gather.10.cloned.1.call-update) | async-done | bytes 11534352 | tf_op jit(solution)/shard_map/all_gather | solution.py:78
  327.6 8.0 %fusion.27 = f32[192,2816]{1,0:T(8,128)} fusion(bf16[192,2048]{1,0:T(8,128)(2,1)S(1)} %all_gather.23, bf16[2048,2816]{1,0:T(8,128)(2,1)} %all-gather.10.cloned.1.call-done), kind=kOutput, calls=%fused_computation.67 | convolution fusion | flops 2214592512 | bytes 14483456 | tf_op jit(solution)/shard_map/dot_general | solution.py:166
  335.7 134.2 %all-gather.12.cloned.1.call-done = bf16[2048,2816]{1,0:T(8,128)(2,1)} async-done(((bf16[128,2816]{1,0:T(8,128)(2,1)}), bf16[2048,2816]{1,0:T(8,128)(2,1)}) %all-gather.12.cloned.1.call-update) | async-done | bytes 11534352 | tf_op jit(solution)/shard_map/all_gather | solution.py:79
  469.9 182.8 %all-gather.14.cloned.1.call-done = bf16[2816,2048]{1,0:T(8,128)(2,1)} async-done(((bf16[2816,128]{1,0:T(8,128)(2,1)}), bf16[2816,2048]{1,0:T(8,128)(2,1)}) %all-gather.14.cloned.1.call-update) | async-done | bytes 11534352 | tf_op jit(solution)/shard_map/all_gather | solution.py:80
  652.7 13.8 %convolution_convert_fusion = bf16[192,2048]{1,0:T(8,128)(2,1)} fusion(bf16[2816,2048]{1,0:T(8,128)(2,1)} %all-gather.14.cloned.1.call-done, bf16[192,2048]{1,0:T(8,128)(2,1)S(1)} %all_gather.23, bf16[2048,2816]{1,0:T(8,128)(2,1)} %all-gather.12.cloned.1.call-done, f32[192,2816]{1,0:T(8,128)} %fusion.27), kind=kOutput, calls=%fused_computation.19 | convolution fusion | flops 4432822272 | bytes 26804224 | tf_op jit(solution)/shard_map/dot_general | solution.py:169
  666.5 6.5 reduce-scatter.5.cloned.1.call-done
  673.0 1.1 fusion.18
  674.1 2.4 all_gather.27
  676.5 0.9 copy.48
  (42 shorter events, 4.9 us)
Async XLA Ops:
  6.5 167.4 %copy-start = (bf16[512,2048]{1,0:T(8,128)(2,1)S(1)}, bf16[512,2048]{1,0:T(8,128)(2,1)}, u32[]{:S(2)}) copy-start(bf16[512,2048]{1,0:T(8,128)(2,1)} %param.18) | copy-start | bytes 6291460
  6.5 64.3 %all-gather.6.cloned.1.call-start = ((), (), s32[]{:S(2)}) async-start(), calls=%async_computation.2 | async-start | bytes 1671168 | tf_op jit(solution)/shard_map/all_gather | solution.py:147
  9.6 120.7 %all-gather.8.cloned.1.call-start = ((), (), s32[]{:S(2)}) async-start(), calls=%async_computation.3 | async-start | bytes 1671168 | tf_op jit(solution)/shard_map/all_gather | solution.py:148
  10.4 172.1 %reduce-scatter.3.cloned.1.call-start = ((), (), s32[]{:S(2)}) async-start(), calls=%async_computation.4 | async-start | bytes 1179648 | tf_op jit(solution)/shard_map/reduce_scatter | solution.py:153
  130.3 53.6 %copy-start.1 = (f32[2048]{0:T(1024)S(1)}, f32[2048]{0:T(1024)}, u32[]{:S(2)}) copy-start(f32[2048]{0:T(1024)} %param.20) | copy-start | bytes 24580
  175.4 152.2 %all-gather.10.cloned.1.call-start = ((), (), s32[]{:S(2)}) async-start(), calls=%async_computation.5 | async-start | bytes 12255232 | tf_op jit(solution)/shard_map/all_gather | solution.py:78
  176.0 293.9 %all-gather.12.cloned.1.call-start = ((), (), s32[]{:S(2)}) async-start(), calls=%async_computation.6 | async-start | bytes 12255232 | tf_op jit(solution)/shard_map/all_gather | solution.py:79
  176.6 476.1 %all-gather.14.cloned.1.call-start = ((), (), s32[]{:S(2)}) async-start(), calls=%async_computation.7 | async-start | bytes 12255232 | tf_op jit(solution)/shard_map/all_gather | solution.py:80
  177.2 495.9 %reduce-scatter.5.cloned.1.call-start = ((), (), s32[]{:S(2)}) async-start(), calls=%async_computation.8 | async-start | bytes 1179648 | tf_op jit(solution)/shard_map/reduce_scatter | solution.py:170
Sparse Core Ops, SparseCore 0:
  10.1 60.6 all-gather.5
  73.6 56.6 all-gather.7
  175.6 6.8 reduce-scatter.2
  185.1 142.5 all-gather.9
  330.2 139.5 all-gather.11
  472.4 180.2 all-gather.13
  666.7 6.3 reduce-scatter.4
where the time goes:
time: 685 us; the launch traced here: 684 us
  waiting for transfers between devices  589 us (86%)
  matrix products  45.1 us (7%)
  other arithmetic  16.4 us (2%)
  local copies, waits for them, and re-layouts  14.7 us (2%)
  between operations  13.7 us (2%)
    all_gather x1, waiting for transfers between devices, body(): lax.all_gather(down_weight, 'sp', axis=1, tiled=True)  183 us
    all_gather x1, waiting for transfers between devices, body(): lax.all_gather(gate_weight, 'sp', axis=0, tiled=True)  141 us
    all_gather x1, waiting for transfers between devices, body(): lax.all_gather(up_weight, 'sp', axis=0, tiled=True)  134 us
    all_gather x1, waiting for transfers between devices, body(): lax.all_gather(values, 'sp', axis=0, tiled=True)  59.5 us
    all_gather x1, waiting for transfers between devices, body(): lax.all_gather(key_turned, 'sp', axis=0, tiled=True)  57.5 us
    dot_general x1, matrix products, body(): terms = jnp.dot(hidden, down_full, preferred_element_type=jnp.float32)  13.8 us
  transfers between devices with their start and end apart: 7, of which 7 were waited for; matrix products, arithmetic and copies ran while one was open for 2% of the time, Pallas kernels for 0%

commit v1 on v0

--- a/solution.py
+++ b/solution.py
@@ -54,6 +54,47 @@
     while length % span != 0:
         span = span - 1
     return span
+
+
+def sub_groups(size, units):
+    ways = 4
+    while size % ways != 0 or units % ways != 0:
+        ways = ways // 2
+    blocks = size // ways
+    lines = [[way * blocks + block for way in range(ways)] for block in range(blocks)]
+    planes = [[way * blocks + block for block in range(blocks)] for way in range(ways)]
+    return ways, lines, planes
+
+
+def swap_blocks(rows, outer, inner):
+    count, width = rows.shape
+    cut = rows.reshape(count, outer, inner, width // (outer * inner))
+    return cut.transpose(0, 2, 1, 3).reshape(count, width)
+
+
+def line_columns(weight, ways, lines):
+    rows, units = weight.shape
+    pieces = weight.reshape(rows, ways, units // ways).transpose(1, 0, 2)
+    line = lax.all_to_all(pieces, "sp", 0, 0, axis_index_groups=lines)
+    return line.reshape(ways * rows, units // ways)
+
+
+def line_rows(weight, ways, lines):
+    units, columns = weight.shape
+    pieces = weight.reshape(ways, units // ways, columns)
+    return lax.all_to_all(pieces, "sp", 0, 0, axis_index_groups=lines)
+
+
+def plane_gather(line, planes):
+    return lax.all_gather(line, "sp", axis=0, tiled=True, axis_index_groups=planes)
+
+
+def gather_pair(keys, values, lines, planes):
+    width = keys.shape[1]
+    both = jnp.concatenate([keys, values], axis=1)
+    line = lax.all_gather(both, "sp", axis=0, tiled=True, axis_index_groups=lines)
+    every = lax.all_gather(line, "sp", axis=0, tiled=True, axis_index_groups=planes)
+    return every[:, :width], every[:, width:]
 
 
 def body(
@@ -74,10 +115,12 @@
     key_heads = key_gain.shape[0]
     head_size = query_gain.shape[1]
     group = heads // key_heads
-    gate_full, up_full, down_full = (
-        lax.all_gather(gate_weight, "sp", axis=0, tiled=True),
-        lax.all_gather(up_weight, "sp", axis=0, tiled=True),
-        lax.all_gather(down_weight, "sp", axis=1, tiled=True),
+    ways, lines, planes = sub_groups(lax.axis_size("sp"), gate_weight.shape[1])
+    gate_line = line_columns(gate_weight, ways, lines)
+    up_line = line_columns(up_weight, ways, lines)
+    down_line = line_rows(down_weight, ways, lines)
+    keys, queries, gate_line, up_line, down_line = lax.optimization_barrier(
+        (keys, queries, gate_line, up_line, down_line)
     )
     places = lax.axis_index("sp") * own + jnp.arange(own, dtype=jnp.int32)
     grid_rows = places // GRID_W
@@ -141,14 +184,17 @@
         jnp.zeros((own, key_heads, group), jnp.float32),
         jnp.zeros((own, key_heads, group, head_size), jnp.float32),
     )
-    top, total, summed = fold_keys(
-        start_state,
-        (
-            lax.all_gather(key_turned, "sp", axis=0, tiled=True),
-            lax.all_gather(values, "sp", axis=0, tiled=True),
-        ),
-    )
+    all_keys, all_values = gather_pair(key_turned, values, lines, planes)
+    all_keys, all_values, gate_line, up_line, down_line = lax.optimization_barrier(
+        (all_keys, all_values, gate_line, up_line, down_line)
+    )
+    gate_full = plane_gather(gate_line, planes)
+    up_full = plane_gather(up_line, planes)
+    down_full = plane_gather(down_line, planes)
+    down_full = down_full.transpose(1, 0, 2).reshape(down_full.shape[1], -1)
+    top, total, summed = fold_keys(start_state, (all_keys, all_values))
     attended = (summed / total[..., None]).reshape(own, heads * head_size).astype(jnp.bfloat16)
+    attended, gate_full, up_full = lax.optimization_barrier((attended, gate_full, up_full))
     part_rows = own // lax.axis_size("tp")
     branch = lax.psum_scatter(
         jnp.dot(
@@ -162,14 +208,22 @@
     ).astype(jnp.float32)
     own_rows = lax.dynamic_slice_in_dim(residual, lax.axis_index("tp") * part_rows, part_rows, 0)
     mid = (own_rows.astype(jnp.float32) + branch).astype(jnp.bfloat16)
-    normed_all = lax.all_gather(row_norm(mid, norm_gain), "tp", axis=0, tiled=True)
+    blocks = lax.axis_size("sp") // ways
+    normed = row_norm(mid, norm_gain)
+    normed = swap_blocks(normed, ways, blocks)
+    normed_line = lax.all_gather(normed, "sp", axis=0, tiled=True, axis_index_groups=lines)
+    normed_all = lax.all_gather(normed_line, "tp", axis=0, tiled=True)
     gate = jnp.dot(normed_all, gate_full, preferred_element_type=jnp.float32)
     up_value = jnp.dot(normed_all, up_full, preferred_element_type=jnp.float32)
     hidden = (jax.nn.silu(gate) * up_value).astype(jnp.bfloat16)
     terms = jnp.dot(hidden, down_full, preferred_element_type=jnp.float32)
+    line_terms = lax.psum_scatter(
+        terms.astype(jnp.bfloat16), "tp", scatter_dimension=0, tiled=True
+    )
     ffn = lax.psum_scatter(
-        terms.astype(jnp.bfloat16), "tp", scatter_dimension=0, tiled=True
+        line_terms, "sp", scatter_dimension=0, tiled=True, axis_index_groups=lines
     ).astype(jnp.float32)
+    ffn = swap_blocks(ffn, blocks, ways)
     finished = (mid.astype(jnp.float32) + ffn).astype(jnp.bfloat16)
     return lax.all_gather(finished, "tp", axis=0, tiled=True)
 

time: 685 us -> 416 us (0.61)
  waiting for transfers between devices: 589 us -> 280 us
  blocking collectives: 4.92 us -> 42 us
  local copies, waits for them, and re-layouts: 14.7 us -> 31 us
  matrix products: 45.1 us -> 30.3 us
  starting transfers between devices: 0.24 us -> 10.4 us
  other arithmetic: 16.4 us -> 8.61 us
    all_gather x5 -> x6, waiting for transfers between devices: 575 us -> 190 us  [the longest x3 97.5 us: plane_gather(): lax.all_gather(line, 'sp', axis=0, tiled=True, axis_index_groups=planes)]
    reduce_scatter x0 -> x1, waiting for transfers between devices: none -> 39.1 us  [body(): lax.psum_scatter(line_terms, 'sp', scatter_dimension=0, tiled=True, axis_...]
    all_to_all x0 -> x2, waiting for transfers between devices: none -> 29.6 us  [the longest x1 17.2 us: line_columns(): line = lax.all_to_all(pieces, 'sp', 0, 0, axis_index_groups=lines)]
    all_to_all x0 -> x1, blocking collectives: none -> 21.4 us  [line_columns(): line = lax.all_to_all(pieces, 'sp', 0, 0, axis_index_groups=lines)]
    all_gather x1, blocking collectives: 2.55 us -> 18.3 us  [gather_pair(): lax.all_gather(both, 'sp', axis=0, tiled=True, axis_index_groups=lines)]
    all_to_all x0 -> x2, starting transfers between devices: none -> 9.84 us  [the longest x1 6.35 us: line_columns(): line = lax.all_to_all(pieces, 'sp', 0, 0, axis_index_groups=lines)]
    reshape x0 -> x8, local copies, waits for them, and re-layouts: none -> 8.7 us  [the longest x4 5.19 us: swap_blocks(): return cut.transpose(0, 2, 1, 3).reshape(count, width)]
    reduce_sum x2, other arithmetic: 10.8 us -> 3.45 us  [absorb(): total = total * shrink + jnp.sum(weight, axis=-1)]
  transfers between devices with their start and end apart: 7 -> 11, of which waited for: 7 -> 11; matrix products, arithmetic and copies ran while one was open for 2% -> 9% of each run, Pallas kernels for 0% -> 0%
where the time goes in v1:
time: 416 us
  waiting for transfers between devices  280 us (67%)
  blocking collectives  42 us (10%)
  local copies, waits for them, and re-layouts  31 us (7%)
  matrix products  30.3 us (7%)
  between operations  13.5 us (3%)
  starting transfers between devices  10.4 us (2%)
  other arithmetic  8.61 us (2%)
    all_gather x3, waiting for transfers between devices, plane_gather(): lax.all_gather(line, 'sp', axis=0, tiled=True, axis_index_groups=planes)  97.5 us
    all_gather x1, waiting for transfers between devices, gather_pair(): lax.all_gather(line, 'sp', axis=0, tiled=True, axis_index_groups=planes)  43 us
    reduce_scatter x1, waiting for transfers between devices, body(): lax.psum_scatter(line_terms, 'sp', scatter_dimension=0, tiled=True, axis_...  39.1 us
    all_gather x1, waiting for transfers between devices, body(): lax.all_gather(normed, 'sp', axis=0, tiled=True, axis_index_groups=lines)  38.2 us
    all_to_all x1, blocking collectives, line_columns(): line = lax.all_to_all(pieces, 'sp', 0, 0, axis_index_groups=lines)  21.4 us
    all_gather x1, blocking collectives, gather_pair(): lax.all_gather(both, 'sp', axis=0, tiled=True, axis_index_groups=lines)  18.3 us
    all_to_all x1, waiting for transfers between devices, line_columns(): line = lax.all_to_all(pieces, 'sp', 0, 0, axis_index_groups=lines)  17.2 us
    dot_general x1, matrix products, body(): terms = jnp.dot(hidden, down_full, preferred_element_type=jnp.float32)  12.4 us
  transfers between devices with their start and end apart: 11, of which 11 were waited for; matrix products, arithmetic and copies ran while one was open for 9% of the time, Pallas kernels for 0%

profile of v1, /device:TPU:0, one launch (start us, length us, event | category | flops | bytes accessed | tf_op | source)
XLA Modules:
  0.0 415.6 jit_solution(11320602952262735499)
XLA Ops:
  6.5 2.4 copy.32
  8.9 6.3 %all-to-all-start = ((bf16[4,128,704]{1,2,0:T(8,128)(2,1)}), bf16[4,128,704]{1,2,0:T(8,128)(2,1)S(1)}, u32[]{:S(2)}, u32[]{:S(2)}) async-start(bf16[4,128,704]{1,2,0:T(8,128)(2,1)} %bitcast.1), calls=%async_computation | async-start | bytes 1441792 | tf_op jit(solution)/shard_map/all_to_all | solution.py:78
  16.7 17.2 %all-to-all-done = bf16[4,128,704]{1,2,0:T(8,128)(2,1)S(1)} async-done(((bf16[4,128,704]{1,2,0:T(8,128)(2,1)}), bf16[4,128,704]{1,2,0:T(8,128)(2,1)S(1)}, u32[]{:S(2)}, u32[]{:S(2)}) %all-to-all-start) | async-done | bytes 720928 | tf_op jit(solution)/shard_map/all_to_all | solution.py:78
  34.0 21.4 %all_to_all.15 = bf16[4,128,704]{1,2,0:T(8,128)(2,1)} all-to-all(bf16[4,128,704]{1,2,0:T(8,128)(2,1)S(1)} %bitcast.107), channel_id=1, replica_groups={{0,8,16,24},{2,10,18,26},{4,12,20,28},{6,14,22,30},{1,9,17,25},{3,11,19..., dimensions={0} | all-to-all | bytes 1441792 | tf_op jit(solution)/shard_map/all_to_all | solution.py:78
  55.3 3.5 all-to-all-start.2
  58.9 1.7 copy.37
  62.4 2.1 copy_bitcast_fusion.1
  64.5 12.3 %all-to-all-done.2 = bf16[4,704,128]{2,1,0:T(8,128)(2,1)S(1)} async-done(((bf16[4,704,128]{2,1,0:T(8,128)(2,1)}), bf16[4,704,128]{2,1,0:T(8,128)(2,1)S(1)}, u32[]{:S(2)}, u32[]{:S(2)}) %all-to-all-start.2) | async-done | bytes 720928 | tf_op jit(solution)/shard_map/all_to_all | solution.py:85
  79.7 18.3 %all_gather.24 = bf16[768,512]{1,0:T(8,128)(2,1)} all-gather(bf16[192,512]{1,0:T(8,128)(2,1)S(1)} %copy.38), channel_id=1, replica_groups={{0,8,16,24},{2,10,18,26},{4,12,20,28},{6,14,22,30},{1,9,17,25},{3,11,19..., dimensions={0}, use_global_device_ids=true | all-gather | bytes 983040 | tf_op jit(solution)/shard_map/all_gather | solution.py:95
  98.2 43.0 %all-gather.7.cloned.1.call-done = bf16[3072,512]{1,0:T(8,128)(2,1)} async-done(((bf16[768,512]{1,0:T(8,128)(2,1)}), bf16[3072,512]{1,0:T(8,128)(2,1)}) %all-gather.7.cloned.1.call-update) | async-done | bytes 3145744 | tf_op jit(solution)/shard_map/all_gather | solution.py:96
  141.2 3.7 fusion.28
  147.3 23.3 %while.15 = (s32[]{:T(128)}, f32[192,4,2]{0,2,1:T(2,128)S(1)}, f32[192,4,2]{0,2,1:T(2,128)S(1)}, f32[192,4,2,64]{0,3,2,1:T(8,128)S(1)}, bf16[2,1536,256]{2,1,0:T...) while((s32[]{:T(128)}, f32[192,4,2]{0,2,1:T(2,128)S(1)}, ...), condition=%wide.region_5.6_spmd.clone, body=%wide.region_2.5_spmd.clone.sunk | while | flops 623156736 | bytes 37257332 | solution.py:179
  147.3 2.4 constant_dynamic-slice_fusion.3
  152.3 2.8 bitcast_reduce_fusion.2
  155.1 1.7 fusion.55
  156.8 2.1 fusion.57
  159.0 2.4 constant_dynamic-slice_fusion.3
  163.9 2.7 bitcast_reduce_fusion.2
  166.7 1.7 fusion.55
  168.4 2.1 fusion.57
  170.7 16.0 %all-gather.9.cloned.1.call-done = bf16[2048,704]{0,1:T(8,128)(2,1)} async-done(((bf16[512,704]{0,1:T(8,128)(2,1)}), bf16[2048,704]{0,1:T(8,128)(2,1)}) %all-gather.9.cloned.1.call-update) | async-done | bytes 2883600 | tf_op jit(solution)/shard_map/all_gather | solution.py:89
  186.6 43.4 %all-gather.11.cloned.1.call-done = bf16[2048,704]{0,1:T(8,128)(2,1)} async-done(((bf16[512,704]{0,1:T(8,128)(2,1)}), bf16[2048,704]{0,1:T(8,128)(2,1)}) %all-gather.11.cloned.1.call-update) | async-done | bytes 2883600 | tf_op jit(solution)/shard_map/all_gather | solution.py:89
  231.6 8.7 %reduce-scatter.4.cloned.1.call-done = bf16[96,2048]{1,0:T(8,128)(2,1)} async-done(((bf16[192,2048]{1,0:T(8,128)(2,1)}), bf16[96,2048]{1,0:T(8,128)(2,1)}) %reduce-scatter.4.cloned.1.call-update) | async-done | bytes 393232 | tf_op jit(solution)/shard_map/reduce_scatter | solution.py:199
  243.3 38.2 %all-gather.13.cloned.1.call-done = bf16[384,2048]{1,0:T(8,128)(2,1)} async-done(((bf16[96,2048]{1,0:T(8,128)(2,1)}), bf16[384,2048]{1,0:T(8,128)(2,1)}) %all-gather.13.cloned.1.call-update) | async-done | bytes 1572880 | tf_op jit(solution)/shard_map/all_gather | solution.py:214
  282.6 11.4 %all-gather.15.cloned.1.call-done = bf16[768,2048]{1,0:T(8,128)(2,1)} async-done(((bf16[384,2048]{1,0:T(8,128)(2,1)}), bf16[768,2048]{1,0:T(8,128)(2,1)}) %all-gather.15.cloned.1.call-update) | async-done | bytes 3145744 | tf_op jit(solution)/shard_map/all_gather | solution.py:215
  294.0 6.6 %fusion.29 = f32[768,704]{0,1:T(8,128)} fusion(bf16[768,2048]{1,0:T(8,128)(2,1)} %all-gather.15.cloned.1.call-done, bf16[2048,704]{0,1:T(8,128)(2,1)} %all-gather.9.cloned.1.call-done), kind=kOutput, calls=%fused_computation.74 | convolution fusion | flops 2214592512 | bytes 8192000 | tf_op jit(solution)/shard_map/dot_general | solution.py:216
  300.6 38.1 %all-gather.17.cloned.1.call-done = bf16[16,704,128]{2,1,0:T(8,128)(2,1)} async-done(((bf16[4,704,128]{2,1,0:T(8,128)(2,1)}), bf16[16,704,128]{2,1,0:T(8,128)(2,1)}) %all-gather.17.cloned.1.call-update) | async-done | bytes 2883600 | tf_op jit(solution)/shard_map/all_gather | solution.py:89
  338.7 12.4 %convolution_convert_fusion = bf16[768,2048]{1,0:T(8,128)(2,1)} fusion(f32[768,704]{0,1:T(8,128)} %fusion.29, bf16[768,2048]{1,0:T(8,128)(2,1)} %all-gather.15.cloned.1.call-done, bf16[2048,704]{0,1:T(8,128)(2,1)} %all-gather.11.cloned.1.call-done, bf16[16,704,128]{2,1,0:T(8,128)(2,1)} %all-gather.17.cloned.1.call-done), kind=kOutput, calls=%fused_computation.17 | convolution fusion | flops 4434001920 | bytes 14221312 | tf_op jit(solution)/shard_map/dot_general | solution.py:219
  351.2 11.3 %reduce-scatter.6.cloned.1.call-done = bf16[384,2048]{1,0:T(8,128)(2,1)} async-done(((bf16[768,2048]{1,0:T(8,128)(2,1)}), bf16[384,2048]{1,0:T(8,128)(2,1)}) %reduce-scatter.6.cloned.1.call-update) | async-done | bytes 1572880 | tf_op jit(solution)/shard_map/reduce_scatter | solution.py:220
  362.5 39.1 %reduce-scatter.8.cloned.1.call-done = bf16[96,2048]{1,0:T(8,128)(2,1)} async-done(((bf16[384,2048]{1,0:T(8,128)(2,1)}), bf16[96,2048]{1,0:T(8,128)(2,1)}) %reduce-scatter.8.cloned.1.call-update) | async-done | bytes 393232 | tf_op jit(solution)/shard_map/reduce_scatter | solution.py:223
  401.5 1.6 reshape.283
  405.8 2.4 all_gather.31
  (80 shorter events, 22.8 us)
Async XLA Ops:
  6.5 223.5 %copy-start = (bf16[512,2048]{1,0:T(8,128)(2,1)S(1)}, bf16[512,2048]{1,0:T(8,128)(2,1)}, u32[]{:S(2)}) copy-start(bf16[512,2048]{1,0:T(8,128)(2,1)} %param.18) | copy-start | bytes 6291460
  8.9 25.1 %all-to-all-start = ((bf16[4,128,704]{1,2,0:T(8,128)(2,1)}), bf16[4,128,704]{1,2,0:T(8,128)(2,1)S(1)}, u32[]{:S(2)}, u32[]{:S(2)}) async-start(bf16[4,128,704]{1,2,0:T(8,128)(2,1)} %bitcast.1), calls=%async_computation | async-start | bytes 1441792 | tf_op jit(solution)/shard_map/all_to_all | solution.py:78
  55.3 21.5 %all-to-all-start.2 = ((bf16[4,704,128]{2,1,0:T(8,128)(2,1)}), bf16[4,704,128]{2,1,0:T(8,128)(2,1)S(1)}, u32[]{:S(2)}, u32[]{:S(2)}) async-start(bf16[4,704,128]{2,1,0:T(8,128)(2,1)} %bitcast.110), calls=%async_computation.2 | async-start | bytes 1441792 | tf_op jit(solution)/shard_map/all_to_all | solution.py:85
  58.8 82.3 %all-gather.7.cloned.1.call-start = ((), (), s32[]{:S(2)}) async-start(), calls=%async_computation.6 | async-start | bytes 3932160 | tf_op jit(solution)/shard_map/all_gather | solution.py:96
  62.4 17.2 %copy-start.2 = (bf16[192,256]{0,1:T(8,128)(2,1)S(1)}, bf16[192,256]{0,1:T(8,128)(2,1)}, u32[]{:S(2)}) copy-start(bf16[192,256]{0,1:T(8,128)(2,1)} %copy.37) | copy-start | bytes 294916
  76.8 68.1 %copy-start.1 = (bf16[4,704,128]{2,1,0:T(8,128)(2,1)}, bf16[4,704,128]{2,1,0:T(8,128)(2,1)S(1)}, u32[]{:S(2)}) copy-start(bf16[4,704,128]{2,1,0:T(8,128)(2,1)S(1)} %all-to-all-done.2) | copy-start | bytes 2162692
  98.1 48.1 %copy-start.8 = (f32[8,64]{1,0:T(8,128)S(1)}, f32[8,64]{1,0:T(8,128)}, u32[]{:S(2)}) copy-start(f32[8,64]{1,0:T(8,128)} %param.16) | copy-start | bytes 6148
  98.1 48.3 %copy-start.4 = (f32[192,16]{0,1:T(8,128)S(1)}, f32[192,16]{0,1:T(8,128)}, u32[]{:S(2)}) copy-start(f32[192,16]{0,1:T(8,128)} %get-tuple-element.146) | copy-start | bytes 36868
  98.1 48.3 %copy-start.5 = (f32[192,16]{0,1:T(8,128)S(1)}, f32[192,16]{0,1:T(8,128)}, u32[]{:S(2)}) copy-start(f32[192,16]{0,1:T(8,128)} %get-tuple-element.149) | copy-start | bytes 36868
  98.1 48.3 %copy-start.6 = (f32[192,16]{0,1:T(8,128)S(1)}, f32[192,16]{0,1:T(8,128)}, u32[]{:S(2)}) copy-start(f32[192,16]{0,1:T(8,128)} %get-tuple-element.150) | copy-start | bytes 36868
  98.1 88.5 %all-gather.9.cloned.1.call-start = ((), (), s32[]{:S(2)}) async-start(), calls=%async_computation.7 | async-start | bytes 3604480 | tf_op jit(solution)/shard_map/all_gather | solution.py:89
  144.9 85.1 %all-gather.11.cloned.1.call-start = ((), (), s32[]{:S(2)}) async-start(), calls=%async_computation.8 | async-start | bytes 3604480 | tf_op jit(solution)/shard_map/all_gather | solution.py:89
  147.2 93.1 %reduce-scatter.4.cloned.1.call-start = ((), (), s32[]{:S(2)}) async-start(), calls=%async_computation.9 | async-start | bytes 1179648 | tf_op jit(solution)/shard_map/reduce_scatter | solution.py:199
  170.6 71.0 %copy-start.7 = (f32[2048]{0:T(1024)S(1)}, f32[2048]{0:T(1024)}, u32[]{:S(2)}) copy-start(f32[2048]{0:T(1024)} %param.20) | copy-start | bytes 24580
  170.6 69.7 %copy-start.3 = (bf16[192,2048]{1,0:T(8,128)(2,1)S(1)}, bf16[192,2048]{1,0:T(8,128)(2,1)}, u32[]{:S(2)}) copy-start(bf16[192,2048]{1,0:T(8,128)(2,1)} %param.19) | copy-start | bytes 2359300
  231.6 50.0 %all-gather.13.cloned.1.call-start = ((), (), s32[]{:S(2)}) async-start(), calls=%async_computation.10 | async-start | bytes 1966080 | tf_op jit(solution)/shard_map/all_gather | solution.py:214
  243.3 50.7 %all-gather.15.cloned.1.call-start = ((), (), s32[]{:S(2)}) async-start(), calls=%async_computation.11 | async-start | bytes 4718592 | tf_op jit(solution)/shard_map/all_gather | solution.py:215
  281.6 57.1 %all-gather.17.cloned.1.call-start = ((), (), s32[]{:S(2)}) async-start(), calls=%async_computation.12 | async-start | bytes 3604480 | tf_op jit(solution)/shard_map/all_gather | solution.py:89
  282.3 80.1 %reduce-scatter.6.cloned.1.call-start = ((), (), s32[]{:S(2)}) async-start(), calls=%async_computation.13 | async-start | bytes 4718592 | tf_op jit(solution)/shard_map/reduce_scatter | solution.py:220
  351.1 50.4 %reduce-scatter.8.cloned.1.call-start = ((), (), s32[]{:S(2)}) async-start(), calls=%async_computation.14 | async-start | bytes 1966080 | tf_op jit(solution)/shard_map/reduce_scatter | solution.py:223
Sparse Core Ops, SparseCore 0:
  98.2 42.9 all-gather.6
  145.1 41.5 all-gather.8
  188.5 41.5 all-gather.10
  232.1 8.1 reduce-scatter.3
  243.4 38.1 all-gather.12
  283.0 10.9 all-gather.14
  295.8 42.8 all-gather.16
  351.3 11.1 reduce-scatter.5
  364.8 36.7 reduce-scatter.7

commit v2 on v1

--- a/solution.py
+++ b/solution.py
@@ -89,12 +89,9 @@
     return lax.all_gather(line, "sp", axis=0, tiled=True, axis_index_groups=planes)
 
 
-def gather_pair(keys, values, lines, planes):
-    width = keys.shape[1]
+def gather_pair(keys, values, lines):
     both = jnp.concatenate([keys, values], axis=1)
-    line = lax.all_gather(both, "sp", axis=0, tiled=True, axis_index_groups=lines)
-    every = lax.all_gather(line, "sp", axis=0, tiled=True, axis_index_groups=planes)
-    return every[:, :width], every[:, width:]
+    return lax.all_gather(both, "sp", axis=0, tiled=True, axis_index_groups=lines)
 
 
 def body(
@@ -116,12 +113,6 @@
     head_size = query_gain.shape[1]
     group = heads // key_heads
     ways, lines, planes = sub_groups(lax.axis_size("sp"), gate_weight.shape[1])
-    gate_line = line_columns(gate_weight, ways, lines)
-    up_line = line_columns(up_weight, ways, lines)
-    down_line = line_rows(down_weight, ways, lines)
-    keys, queries, gate_line, up_line, down_line = lax.optimization_barrier(
-        (keys, queries, gate_line, up_line, down_line)
-    )
     places = lax.axis_index("sp") * own + jnp.arange(own, dtype=jnp.int32)
     grid_rows = places // GRID_W
     grid_cols = places % GRID_W
@@ -184,7 +175,15 @@
         jnp.zeros((own, key_heads, group), jnp.float32),
         jnp.zeros((own, key_heads, group, head_size), jnp.float32),
     )
-    all_keys, all_values = gather_pair(key_turned, values, lines, planes)
+    pair_line = gather_pair(key_turned, values, lines)
+    pair_line, gate_weight, up_weight, down_weight = lax.optimization_barrier(
+        (pair_line, gate_weight, up_weight, down_weight)
+    )
+    pair = plane_gather(pair_line, planes)
+    all_keys, all_values = pair[:, : keys.shape[1]], pair[:, keys.shape[1] :]
+    gate_line = line_columns(gate_weight, ways, lines)
+    up_line = line_columns(up_weight, ways, lines)
+    down_line = line_rows(down_weight, ways, lines)
     all_keys, all_values, gate_line, up_line, down_line = lax.optimization_barrier(
         (all_keys, all_values, gate_line, up_line, down_line)
     )

time: 416 us -> 365 us (0.88)
  waiting for transfers between devices: 280 us -> 229 us
    all_gather x1 -> x0, waiting for transfers between devices: 43 us -> none  [gather_pair(): lax.all_gather(line, 'sp', axis=0, tiled=True, axis_index_groups=planes)]
    all_gather x3 -> x4, waiting for transfers between devices: 97.5 us -> 93.9 us  [plane_gather(): lax.all_gather(line, 'sp', axis=0, tiled=True, axis_index_groups=planes)]
  transfers between devices with their start and end apart: 11 -> 11, of which waited for: 11 -> 10; matrix products, arithmetic and copies ran while one was open for 9% -> 12% of each run, Pallas kernels for 0% -> 0%
where the time goes in v2:
time: 365 us; the launch traced here: 364 us
  waiting for transfers between devices  229 us (63%)
  blocking collectives  44.6 us (12%)
  local copies, waits for them, and re-layouts  30.7 us (8%)
  matrix products  30.2 us (8%)
  between operations  13.5 us (4%)
  other arithmetic  9.15 us (3%)
  starting transfers between devices  7.49 us (2%)
    all_gather x4, waiting for transfers between devices, plane_gather(): lax.all_gather(line, 'sp', axis=0, tiled=True, axis_index_groups=planes)  93.9 us
    reduce_scatter x1, waiting for transfers between devices, body(): lax.psum_scatter(line_terms, 'sp', scatter_dimension=0, tiled=True, axis_...  39.1 us
    all_gather x1, waiting for transfers between devices, body(): lax.all_gather(normed, 'sp', axis=0, tiled=True, axis_index_groups=lines)  38.2 us
    all_gather x1, blocking collectives, gather_pair(): lax.all_gather(both, 'sp', axis=0, tiled=True, axis_index_groups=lines)  21.7 us
    all_to_all x1, blocking collectives, line_columns(): line = lax.all_to_all(pieces, 'sp', 0, 0, axis_index_groups=lines)  20.5 us
    all_to_all x1, waiting for transfers between devices, line_columns(): line = lax.all_to_all(pieces, 'sp', 0, 0, axis_index_groups=lines)  14.8 us
    dot_general x1, matrix products, body(): terms = jnp.dot(hidden, down_full, preferred_element_type=jnp.float32)  12.4 us
    all_gather x1, waiting for transfers between devices, body(): normed_all = lax.all_gather(normed_line, 'tp', axis=0, tiled=True)  11.4 us
  transfers between devices with their start and end apart: 11, of which 10 were waited for; matrix products, arithmetic and copies ran while one was open for 12% of the time, Pallas kernels for 0%

profile of v2, /device:TPU:0, one launch (start us, length us, event | category | flops | bytes accessed | tf_op | source)
XLA Modules:
  0.0 364.4 jit_solution(9703807676451618923)
XLA Ops:
  10.6 21.7 %all_gather.24 = bf16[768,512]{1,0:T(8,128)(2,1)} all-gather(bf16[192,512]{1,0:T(8,128)(2,1)S(1)} %copy.34), channel_id=1, replica_groups={{0,8,16,24},{2,10,18,26},{4,12,20,28},{6,14,22,30},{1,9,17,25},{3,11,19..., dimensions={0}, use_global_device_ids=true | all-gather | bytes 983040 | tf_op jit(solution)/shard_map/all_gather | solution.py:94
  33.5 3.5 all-to-all-start
  37.0 1.5 copy.37
  38.5 14.8 %all-to-all-done = bf16[4,128,704]{1,2,0:T(8,128)(2,1)S(1)} async-done(((bf16[4,128,704]{1,2,0:T(8,128)(2,1)}), bf16[4,128,704]{1,2,0:T(8,128)(2,1)S(1)}, u32[]{:S(2)}, u32[]{:S(2)}) %all-to-all-start) | async-done | bytes 720928 | tf_op jit(solution)/shard_map/all_to_all | solution.py:78
  53.3 20.5 %all_to_all.15 = bf16[4,128,704]{1,2,0:T(8,128)(2,1)} all-to-all(bf16[4,128,704]{1,2,0:T(8,128)(2,1)S(1)} %bitcast.107), channel_id=1, replica_groups={{0,8,16,24},{2,10,18,26},{4,12,20,28},{6,14,22,30},{1,9,17,25},{3,11,19..., dimensions={0} | all-to-all | bytes 1441792 | tf_op jit(solution)/shard_map/all_to_all | solution.py:78
  73.8 3.5 all-to-all-start.2
  78.4 2.0 copy_bitcast_fusion.1
  80.5 3.8 %fusion.28 = (bf16[3072,256]{1,0:T(8,128)(2,1)}, bf16[3072,256]{1,0:T(8,128)(2,1)}) fusion(bf16[3072,512]{1,0:T(8,128)(2,1)} %all-gather.7.cloned.1.call-done), kind=kLoop, calls=%fused_computation.73 | loop fusion | bytes 6291456 | tf_op jit(solution)/shard_map/slice | solution.py:183
  84.2 10.4 %all-to-all-done.2 = bf16[4,704,128]{2,1,0:T(8,128)(2,1)S(1)} async-done(((bf16[4,704,128]{2,1,0:T(8,128)(2,1)}), bf16[4,704,128]{2,1,0:T(8,128)(2,1)S(1)}, u32[]{:S(2)}, u32[]{:S(2)}) %all-to-all-start.2) | async-done | bytes 720928 | tf_op jit(solution)/shard_map/all_to_all | solution.py:85
  94.7 1.9 copy.39
  99.8 23.3 %while.15 = (s32[]{:T(128)}, f32[192,4,2]{0,2,1:T(2,128)S(1)}, f32[192,4,2]{0,2,1:T(2,128)S(1)}, f32[192,4,2,64]{0,3,2,1:T(8,128)S(1)}, bf16[2,1536,256]{2,1,0:T...) while((s32[]{:T(128)}, f32[192,4,2]{0,2,1:T(2,128)S(1)}, ...), condition=%wide.region_5.6_spmd.clone, body=%wide.region_2.5_spmd.clone.sunk | while | flops 623156736 | bytes 37257332 | solution.py:170
  99.8 2.5 constant_dynamic-slice_fusion.3
  104.8 2.7 bitcast_reduce_fusion.2
  107.6 1.7 fusion.55
  109.3 2.1 fusion.57
  111.5 2.4 constant_dynamic-slice_fusion.3
  116.4 2.7 bitcast_reduce_fusion.2
  119.2 1.7 fusion.55
  120.9 2.1 fusion.57
  123.2 12.3 %all-gather.9.cloned.1.call-done = bf16[2048,704]{0,1:T(8,128)(2,1)} async-done(((bf16[512,704]{0,1:T(8,128)(2,1)}), bf16[2048,704]{0,1:T(8,128)(2,1)}) %all-gather.9.cloned.1.call-update) | async-done | bytes 2883600 | tf_op jit(solution)/shard_map/all_gather | solution.py:89
  135.5 43.4 %all-gather.11.cloned.1.call-done = bf16[2048,704]{0,1:T(8,128)(2,1)} async-done(((bf16[512,704]{0,1:T(8,128)(2,1)}), bf16[2048,704]{0,1:T(8,128)(2,1)}) %all-gather.11.cloned.1.call-update) | async-done | bytes 2883600 | tf_op jit(solution)/shard_map/all_gather | solution.py:89
  178.9 1.5 convolution_convert_fusion.1
  180.4 8.7 %reduce-scatter.4.cloned.1.call-done = bf16[96,2048]{1,0:T(8,128)(2,1)} async-done(((bf16[192,2048]{1,0:T(8,128)(2,1)}), bf16[96,2048]{1,0:T(8,128)(2,1)}) %reduce-scatter.4.cloned.1.call-update) | async-done | bytes 393232 | tf_op jit(solution)/shard_map/reduce_scatter | solution.py:198
  192.1 38.2 %all-gather.13.cloned.1.call-done = bf16[384,2048]{1,0:T(8,128)(2,1)} async-done(((bf16[96,2048]{1,0:T(8,128)(2,1)}), bf16[384,2048]{1,0:T(8,128)(2,1)}) %all-gather.13.cloned.1.call-update) | async-done | bytes 1572880 | tf_op jit(solution)/shard_map/all_gather | solution.py:213
  231.4 11.4 %all-gather.15.cloned.1.call-done = bf16[768,2048]{1,0:T(8,128)(2,1)} async-done(((bf16[384,2048]{1,0:T(8,128)(2,1)}), bf16[768,2048]{1,0:T(8,128)(2,1)}) %all-gather.15.cloned.1.call-update) | async-done | bytes 3145744 | tf_op jit(solution)/shard_map/all_gather | solution.py:214
  242.8 6.6 %fusion.29 = f32[768,704]{0,1:T(8,128)} fusion(bf16[768,2048]{1,0:T(8,128)(2,1)} %all-gather.15.cloned.1.call-done, bf16[2048,704]{0,1:T(8,128)(2,1)} %all-gather.9.cloned.1.call-done), kind=kOutput, calls=%fused_computation.74 | convolution fusion | flops 2214592512 | bytes 8192000 | tf_op jit(solution)/shard_map/dot_general | solution.py:215
  249.4 38.1 %all-gather.17.cloned.1.call-done = bf16[16,704,128]{2,1,0:T(8,128)(2,1)} async-done(((bf16[4,704,128]{2,1,0:T(8,128)(2,1)}), bf16[16,704,128]{2,1,0:T(8,128)(2,1)}) %all-gather.17.cloned.1.call-update) | async-done | bytes 2883600 | tf_op jit(solution)/shard_map/all_gather | solution.py:89
  287.5 12.4 %convolution_convert_fusion = bf16[768,2048]{1,0:T(8,128)(2,1)} fusion(f32[768,704]{0,1:T(8,128)} %fusion.29, bf16[768,2048]{1,0:T(8,128)(2,1)} %all-gather.15.cloned.1.call-done, bf16[2048,704]{0,1:T(8,128)(2,1)} %all-gather.11.cloned.1.call-done, bf16[16,704,128]{2,1,0:T(8,128)(2,1)} %all-gather.17.cloned.1.call-done), kind=kOutput, calls=%fused_computation.17 | convolution fusion | flops 4434001920 | bytes 14221312 | tf_op jit(solution)/shard_map/dot_general | solution.py:218
  300.0 11.3 %reduce-scatter.6.cloned.1.call-done = bf16[384,2048]{1,0:T(8,128)(2,1)} async-done(((bf16[768,2048]{1,0:T(8,128)(2,1)}), bf16[384,2048]{1,0:T(8,128)(2,1)}) %reduce-scatter.6.cloned.1.call-update) | async-done | bytes 1572880 | tf_op jit(solution)/shard_map/reduce_scatter | solution.py:219
  311.3 39.1 %reduce-scatter.8.cloned.1.call-done = bf16[96,2048]{1,0:T(8,128)(2,1)} async-done(((bf16[384,2048]{1,0:T(8,128)(2,1)}), bf16[96,2048]{1,0:T(8,128)(2,1)}) %reduce-scatter.8.cloned.1.call-update) | async-done | bytes 393232 | tf_op jit(solution)/shard_map/reduce_scatter | solution.py:222
  350.4 1.6 reshape.283
  354.6 2.4 all_gather.31
  (86 shorter events, 22.1 us)
Async XLA Ops:
  6.5 172.3 %copy-start = (bf16[512,2048]{1,0:T(8,128)(2,1)S(1)}, bf16[512,2048]{1,0:T(8,128)(2,1)}, u32[]{:S(2)}) copy-start(bf16[512,2048]{1,0:T(8,128)(2,1)} %param.18) | copy-start | bytes 6291460
  6.5 25.8 %copy-start.2 = (bf16[128,2816]{1,0:T(8,128)(2,1)S(1)}, bf16[128,2816]{1,0:T(8,128)(2,1)}, u32[]{:S(2)}) copy-start(bf16[128,2816]{1,0:T(8,128)(2,1)} %param.21) | copy-start | bytes 2162692
  6.5 73.9 %all-gather.7.cloned.1.call-start = ((), (), s32[]{:S(2)}) async-start(), calls=%async_computation.6 | async-start | bytes 3932160 | tf_op jit(solution)/shard_map/all_gather | solution.py:89
  9.8 0.6 copy-start.4
  9.8 0.6 copy-start.6
  9.8 0.6 copy-start.8
  33.5 19.8 %all-to-all-start = ((bf16[4,128,704]{1,2,0:T(8,128)(2,1)}), bf16[4,128,704]{1,2,0:T(8,128)(2,1)S(1)}, u32[]{:S(2)}, u32[]{:S(2)}) async-start(bf16[4,128,704]{1,2,0:T(8,128)(2,1)} %bitcast.4), calls=%async_computation | async-start | bytes 1441792 | tf_op jit(solution)/shard_map/all_to_all | solution.py:78
  73.8 20.8 %all-to-all-start.2 = ((bf16[4,704,128]{2,1,0:T(8,128)(2,1)}), bf16[4,704,128]{2,1,0:T(8,128)(2,1)S(1)}, u32[]{:S(2)}, u32[]{:S(2)}) async-start(bf16[4,704,128]{2,1,0:T(8,128)(2,1)} %bitcast.110), calls=%async_computation.2 | async-start | bytes 1441792 | tf_op jit(solution)/shard_map/all_to_all | solution.py:85
  77.3 58.2 %all-gather.9.cloned.1.call-start = ((), (), s32[]{:S(2)}) async-start(), calls=%async_computation.7 | async-start | bytes 3604480 | tf_op jit(solution)/shard_map/all_gather | solution.py:89
  80.4 17.3 %copy-start.11 = (f32[8,64]{1,0:T(8,128)S(1)}, f32[8,64]{1,0:T(8,128)}, u32[]{:S(2)}) copy-start(f32[8,64]{1,0:T(8,128)} %param.16) | copy-start | bytes 6148
  80.4 18.4 %copy-start.5 = (f32[192,16]{0,1:T(8,128)S(1)}, f32[192,16]{0,1:T(8,128)}, u32[]{:S(2)}) copy-start(f32[192,16]{0,1:T(8,128)} %copy-done.4) | copy-start | bytes 36868
  80.4 18.4 %copy-start.7 = (f32[192,16]{0,1:T(8,128)S(1)}, f32[192,16]{0,1:T(8,128)}, u32[]{:S(2)}) copy-start(f32[192,16]{0,1:T(8,128)} %copy-done.6) | copy-start | bytes 36868
  80.4 18.4 %copy-start.9 = (f32[192,16]{0,1:T(8,128)S(1)}, f32[192,16]{0,1:T(8,128)}, u32[]{:S(2)}) copy-start(f32[192,16]{0,1:T(8,128)} %copy-done.8) | copy-start | bytes 36868
  94.6 5.1 %copy-start.1 = (bf16[4,704,128]{2,1,0:T(8,128)(2,1)}, bf16[4,704,128]{2,1,0:T(8,128)(2,1)S(1)}, u32[]{:S(2)}) copy-start(bf16[4,704,128]{2,1,0:T(8,128)(2,1)S(1)} %all-to-all-done.2) | copy-start | bytes 2162692
  94.7 84.2 %all-gather.11.cloned.1.call-start = ((), (), s32[]{:S(2)}) async-start(), calls=%async_computation.8 | async-start | bytes 3604480 | tf_op jit(solution)/shard_map/all_gather | solution.py:89
  99.7 89.5 %reduce-scatter.4.cloned.1.call-start = ((), (), s32[]{:S(2)}) async-start(), calls=%async_computation.9 | async-start | bytes 1179648 | tf_op jit(solution)/shard_map/reduce_scatter | solution.py:198
  123.1 67.3 %copy-start.10 = (f32[2048]{0:T(1024)S(1)}, f32[2048]{0:T(1024)}, u32[]{:S(2)}) copy-start(f32[2048]{0:T(1024)} %param.20) | copy-start | bytes 24580
  123.1 66.0 %copy-start.3 = (bf16[192,2048]{1,0:T(8,128)(2,1)S(1)}, bf16[192,2048]{1,0:T(8,128)(2,1)}, u32[]{:S(2)}) copy-start(bf16[192,2048]{1,0:T(8,128)(2,1)} %param.19) | copy-start | bytes 2359300
  180.4 50.0 %all-gather.13.cloned.1.call-start = ((), (), s32[]{:S(2)}) async-start(), calls=%async_computation.10 | async-start | bytes 1966080 | tf_op jit(solution)/shard_map/all_gather | solution.py:213
  192.1 50.7 %all-gather.15.cloned.1.call-start = ((), (), s32[]{:S(2)}) async-start(), calls=%async_computation.11 | async-start | bytes 4718592 | tf_op jit(solution)/shard_map/all_gather | solution.py:214
  230.4 57.1 %all-gather.17.cloned.1.call-start = ((), (), s32[]{:S(2)}) async-start(), calls=%async_computation.12 | async-start | bytes 3604480 | tf_op jit(solution)/shard_map/all_gather | solution.py:89
  231.2 80.1 %reduce-scatter.6.cloned.1.call-start = ((), (), s32[]{:S(2)}) async-start(), calls=%async_computation.13 | async-start | bytes 4718592 | tf_op jit(solution)/shard_map/reduce_scatter | solution.py:219
  300.0 50.4 %reduce-scatter.8.cloned.1.call-start = ((), (), s32[]{:S(2)}) async-start(), calls=%async_computation.14 | async-start | bytes 1966080 | tf_op jit(solution)/shard_map/reduce_scatter | solution.py:222
Sparse Core Ops, SparseCore 0:
  32.5 43.4 all-gather.6
  94.8 40.6 all-gather.8
  137.3 41.5 all-gather.10
  181.0 8.1 reduce-scatter.3
  192.2 38.1 all-gather.12
  231.8 10.9 all-gather.14
  244.6 42.8 all-gather.16
  300.1 11.1 reduce-scatter.5
  313.6 36.7 reduce-scatter.7
